TPU v7x, 32 devices: a whole 2x2x4 slice. The times are simulated.
32 devices in a mesh: sp: 16 (over z, y, x), tp: 2 (over core).
Axes of the slice: x: 2, y: 2, z: 4, core: 2. Of those that a mesh axis runs over, the one named last changes fastest.
Arguments:
- query_one: bfloat16 [2048, 1024], P('sp', 'tp'), may hold values from -85 to 85
- key_one: bfloat16 [2048, 1024], P('sp', 'tp'), may hold values from -6.5 to 6.5
- query_two: bfloat16 [2048, 1024], P('sp', 'tp'), may hold values from -85 to 85
- key_two: bfloat16 [2048, 1024], P('sp', 'tp'), may hold values from -6.5 to 6.5
- values: bfloat16 [2048, 2048], P('sp', 'tp'), may hold values from -6 to 6
- mix_weight: float32 [8], P('tp'), may hold values from 0.3 to 0.8
- head_gain: float32 [256], replicated, may hold values from 0.1 to 1.9
- residual: bfloat16 [2048, 2048], P(('sp', 'tp')), may hold values from -6 to 6
- out_weight: bfloat16 [2048, 2048], P('tp'), may hold values from -0.125 to 0.125
- norm_gain: float32 [2048], replicated, may hold values from 0.1 to 1.9
- lift_weight: bfloat16 [2048, 5632], P('sp', 'tp'), may hold values from -0.125 to 0.125
- gate_weight: bfloat16 [2048, 5632], P('sp', 'tp'), may hold values from -0.125 to 0.125
- conv_taps: float32 [3, 5632], P(None, 'tp'), may hold values from -3 to 3
- down_weight: bfloat16 [5632, 2048], P('tp'), may hold values from -0.078125 to 0.078125
Outputs:
- layer_out: bfloat16 [2048, 2048], P(('sp', 'tp'))
All inputs are finite; a program needn't handle non-finite values.
Results may differ from a plain program's by a relative error of at most 0.015.
Values may be sent and summed in bfloat16 or wider, within the bound.
A program may use at most 128 MiB of HBM per device.

v0:
```python
import functools

import jax
import jax.numpy as jnp
from jax import lax
from jax.experimental import pallas as pl
from jax.experimental.pallas import tpu as pltpu
from jax.sharding import PartitionSpec as P

HD = 128
STRETCH = 64
WIDTH = 3


epsilon = 1e-06
masked_score = -1e30


def passed_along(block, axis, distance):
    devices = range(lax.axis_size(axis))
    route = [(i - distance, i) for i in devices if i - distance in devices]
    return lax.ppermute(block, axis, route)


def update_map(peak, total, acc, queries, keys, vals, visible):
    scores = jnp.einsum("thd,shd->hts", queries, keys, preferred_element_type=jnp.float32) * HD ** (
        -0.5
    )
    scores = jnp.where(visible[None], scores, masked_score)
    new_peak = jnp.maximum(peak, jnp.max(scores, axis=-1))
    weights = jnp.where(visible[None], jnp.exp(scores - new_peak[..., None]), 0.0)
    total = jnp.sum(weights, axis=-1)
    acc = jnp.einsum(
        "hts,she->hte", weights.astype(jnp.bfloat16), vals, preferred_element_type=jnp.float32
    )
    return (new_peak, total, acc)


def on_device(
    query_one,
    key_one,
    query_two,
    key_two,
    values,
    mix_weight,
    head_gain,
    residual,
    out_weight,
    norm_gain,
    lift_weight,
    gate_weight,
    conv_taps,
    down_weight,
):
    tok_local = query_one.shape[0]
    heads_local = mix_weight.shape[0]
    val_width = values.shape[1] // heads_local
    model_width = residual.shape[1]
    offset = lax.axis_index("sp") * tok_local
    q_pos = offset + lax.iota(jnp.int32, tok_local)
    q_one = query_one.reshape(tok_local, heads_local, HD)
    q_two = query_two.reshape(tok_local, heads_local, HD)
    start_peak = jnp.full((heads_local, tok_local), masked_score, jnp.float32)
    start_total = jnp.zeros((heads_local, tok_local), jnp.float32)
    start_acc = jnp.zeros((heads_local, tok_local, val_width), jnp.float32)
    initial = (start_peak, start_total, start_acc, start_peak, start_total, start_acc)
    first_keys = lax.all_gather(key_one, "sp", axis=0, tiled=True)
    second_keys = lax.all_gather(key_two, "sp", axis=0, tiled=True)
    piece_vals = lax.all_gather(values, "sp", axis=0, tiled=True)
    count = first_keys.shape[0]
    k_pos = lax.iota(jnp.int32, count)
    visible = k_pos[None, :] // STRETCH <= q_pos[:, None] // STRETCH
    first_keys = first_keys.reshape(count, heads_local, HD)
    second_keys = second_keys.reshape(count, heads_local, HD)
    piece_vals = piece_vals.reshape(count, heads_local, val_width)
    first = update_map(initial[0], initial[1], initial[2], q_one, first_keys, piece_vals, visible)
    second = update_map(initial[3], initial[4], initial[5], q_two, second_keys, piece_vals, visible)
    state = first + second
    mixed = (
        state[2] / state[1][..., None] - mix_weight[:, None, None] * state[5] / state[4][..., None]
    )
    head_out = (
        mixed * lax.rsqrt(jnp.mean(mixed * mixed, axis=-1, keepdims=True) + epsilon) * head_gain
    ).astype(jnp.bfloat16)
    out_heads = out_weight.reshape(heads_local, val_width, model_width)
    piece = head_out
    attended = lax.psum_scatter(
        jnp.einsum("hte,hed->td", piece, out_heads, preferred_element_type=jnp.float32).astype(
            jnp.bfloat16
        ),
        "tp",
        scatter_dimension=0,
        tiled=True,
    ).astype(jnp.float32)
    stream = residual.astype(jnp.float32) + attended
    normed = (
        stream * lax.rsqrt(jnp.mean(stream * stream, axis=-1, keepdims=True) + epsilon) * norm_gain
    ).astype(jnp.bfloat16)
    whole_rows = lax.all_gather(normed, "tp", axis=0, tiled=True)
    lift_pre = jnp.dot(
        whole_rows,
        lax.all_gather(lift_weight, "sp", axis=0, tiled=True),
        preferred_element_type=jnp.float32,
    )
    gate_pre = jnp.dot(
        whole_rows,
        lax.all_gather(gate_weight, "sp", axis=0, tiled=True),
        preferred_element_type=jnp.float32,
    )
    lifted = lift_pre.astype(jnp.bfloat16)
    gated = gate_pre.astype(jnp.bfloat16)
    prior = passed_along(gated[tok_local - (WIDTH - 1) :], "sp", 1)
    extended = jnp.concatenate([prior, gated], axis=0).astype(jnp.float32)
    conv = conv_taps[0] * extended[0:tok_local]
    for index in range(1, WIDTH):
        conv = conv + conv_taps[index] * extended[index : index + tok_local]
    hidden = (jax.nn.silu(conv) * lifted.astype(jnp.float32)).astype(jnp.bfloat16)
    piece = hidden
    mixer = lax.psum_scatter(
        jnp.dot(piece, down_weight, preferred_element_type=jnp.float32).astype(jnp.bfloat16),
        "tp",
        scatter_dimension=0,
        tiled=True,
    ).astype(jnp.float32)
    return (stream + mixer).astype(jnp.bfloat16)

MESH = pl.DeviceIdType.MESH


def remote(src, dst, send_sem, recv_sem, sp, tp):
    return pltpu.make_async_remote_copy(
        src_ref=src,
        dst_ref=dst,
        send_sem=send_sem,
        recv_sem=recv_sem,
        device_id=(sp, tp),
        device_id_type=MESH,
    )


def greet(peers, count=None):
    barrier = pltpu.get_barrier_semaphore()
    for peer in peers:
        pl.semaphore_signal(barrier, inc=1, device_id=peer, device_id_type=MESH)
    pl.semaphore_wait(barrier, len(peers) if count is None else count)


def block_of(index, size):
    return pl.ds(pl.multiple_of(index * size, size), size)


def front_kernel(
    plane, planes, width, q1, k1, q2, k2, v, lift, gate, mix_weight, head_gain, out_hbm, residual_hbm,
    gain,
    lift_all, gate_all, normed, halo, stream,
    q_all, kv_all, peaks, totals, sums, head_out, heads, part, part_in, tail, out_weight, residual,
    own_sem, a_send, a_recv, w_send, w_recv, kv_send, kv_recv, g_send, g_recv,
    b_own, b_send, b_recv, t_send, t_recv, up_send, up_recv, down_send, down_recv,
    f_send, f_recv, h_send, h_recv,
):
    sp, tp = lax.axis_index("sp"), lax.axis_index("tp")
    z, p = sp // plane, sp % plane
    other = 1 - tp
    tok = q1.shape[0]
    half = tok // 2
    val = 2 * HD
    tiles = lift.shape[1] // 128
    before = (p + plane - 1) % plane
    above, below = (z + 1) % planes * plane + p, (z + planes - 1) % planes * plane + p
    weights = ((lift, lift_all), (gate, gate_all))
    peers = (
        [(z * plane + (p + d) % plane, tp) for d in range(1, plane)]
        + [((z + d) % planes * plane + p, tp) for d in range(1, planes)]
        + [(sp, other)]
    )
    barrier = pltpu.get_barrier_semaphore()
    for peer in peers + [(s * plane + before, 1) for s in range(planes)]:
        pl.semaphore_signal(barrier, inc=1, device_id=peer, device_id_type=MESH)

    def piece(head, row):
        h1, h2 = block_of(head, HD), block_of(head, 2 * HD)
        rows, all_rows = block_of(row % plane, tok), block_of(row, tok)
        return [
            (k1.at[:, h1], kv_all.at[all_rows, 0:HD]),
            (k2.at[:, h1], kv_all.at[all_rows, HD : 2 * HD]),
            (v.at[:, h2], kv_all.at[all_rows, 2 * HD : 4 * HD]),
            (q1.at[:, h1], q_all.at[rows, 0:HD]),
            (q2.at[:, h1], q_all.at[rows, HD : 2 * HD]),
        ]

    def units(index):
        return pl.ds(pl.multiple_of(index * tiles // planes * 128, 128), width)

    started = []
    own = [
        pltpu.make_async_copy(src, dst, own_sem.at[n]) for n, (src, dst) in enumerate(piece(p, sp))
    ]
    own_weights = [
        pltpu.make_async_copy(src.at[:, units(z)], dst.at[block_of(sp, tok), :], own_sem.at[5 + m])
        for m, (src, dst) in enumerate(weights)
    ]
    for copy in own:
        copy.start()
    loads = [
        pltpu.make_async_copy(out_hbm, out_weight, own_sem.at[7]),
        pltpu.make_async_copy(residual_hbm, residual, own_sem.at[8]),
    ]
    pl.semaphore_wait(barrier, len(peers) + 2 * planes * tp)
    for part_of in ((0, 1, 2), (3, 4)):
        for d in range(1, plane):
            there = (p + d) % plane
            pairs = piece(there, sp)
            for n in part_of:
                src, dst = pairs[n]
                copy = remote(src, dst, a_send.at[d, n], a_recv.at[d, n], z * plane + there, tp)
                copy.start()
                started.append(copy)

    lanes = {}
    for d in range(1, planes):
        there = (z + d) % planes
        lanes[d] = [
            remote(
                src.at[:, units(there)], dst.at[block_of(sp, tok), :],
                w_send.at[d, m], w_recv.at[d, m], there * plane + p, tp,
            )
            for m, (src, dst) in enumerate(weights)
        ]
        started.extend(lanes[d])

    def send_weights(early):
        for d in range(planes - 1, 0, -1):

            if d == planes - 1:
                turn = (z > 0) if early else None
            else:
                turn = (z + d >= planes) if early else (z + d < planes)
            if turn is None:
                continue

            @pl.when(turn)
            def _():
                for copy in lanes[d]:
                    copy.start()

    square = plane == 4
    direct = (1, 2) if square else range(1, plane)

    def partner(e):
        if not square:
            return (p + e) % plane
        flips = {1: p + 1 - 2 * (p % 2), 2: (p + 2) % 4, 3: 3 - p}
        return flips[e]

    def share_weights(d):
        source = (z + planes - d) % planes * plane + p
        rows = block_of(source, tok)
        for m, dst in enumerate((lift_all, gate_all)):
            if d:
                remote(
                    dst.at[rows, :], dst.at[rows, :], w_send.at[d, m], w_recv.at[d, m], source, tp
                ).wait_recv()
            src = dst.at[rows, :] if d else weights[m][0].at[:, units(z)]
            for e in direct:
                copy = remote(
                    src, dst.at[rows, :], g_send.at[d, e, m], g_recv.at[d, e, m],
                    z * plane + partner(e), tp,
                )
                copy.start()
                started.append(copy)

    def pass_weights(d):
        for m, dst in enumerate((lift_all, gate_all)):
            for e in direct:
                there = partner(e) if square else (p + plane - e) % plane
                rows = block_of((z + planes - d) % planes * plane + there, tok)
                block = dst.at[rows, :]
                remote(
                    block, block, g_send.at[d, e, m], g_recv.at[d, e, m], z * plane + there, tp
                ).wait_recv()
                if square and e == m + 1:
                    copy = remote(
                        block, block, g_send.at[d, 3, m], g_recv.at[d, 3, m],
                        z * plane + partner(3 - e), tp,
                    )
                    copy.start()
                    started.append(copy)

    send_weights(True)
    share_weights(0)
    for copy in own_weights + loads:
        copy.start()
    span = plane * tok

    def keys_of(index, e):
        return kv_all.at[block_of(index * plane + (p + plane - e) % plane, tok), :]

    def arrival(e, which):
        source = z * plane + (p + plane - e) % plane
        pairs = piece(p, source)
        for n in which:
            src, dst = pairs[n]
            remote(src, dst, a_send.at[e, n], a_recv.at[e, n], source, tp).wait_recv()

    for e in range(plane):
        if e:
            arrival(e, (0, 1, 2))
        else:
            for copy in own[:3]:
                copy.wait()

        @pl.when(z + 1 < planes)
        def _():
            block = keys_of(z, e)
            remote(block, block, kv_send.at[1, e], kv_recv.at[1, e], above, tp).start()

    @pl.when(z == 0)
    def _():
        for copy in lanes[planes - 1]:
            copy.start()

    for copy in own[3:]:
        copy.wait()
    for e in range(1, plane):
        arrival(e, (3, 4))

    def attend(source, first):
        @pl.loop(0, plane)
        def _(chunk):
            rows, keys = block_of(chunk, tok), block_of(source, span)
            for m in range(2):
                scores = lax.dot_general(
                    q_all[rows, m * HD : (m + 1) * HD],
                    kv_all[keys, m * HD : (m + 1) * HD],
                    (((1,), (1,)), ((), ())),
                    preferred_element_type=jnp.float32,
                ) * HD ** (-0.5)
                if first:
                    k_pos = lax.broadcasted_iota(jnp.int32, (tok, span), 1)
                    q_pos = chunk * tok + lax.broadcasted_iota(jnp.int32, (tok, span), 0)
                    visible = lax.div(k_pos, STRETCH) <= lax.div(q_pos, STRETCH)
                    scores = jnp.where(visible, scores, masked_score)
                    peak = jnp.max(scores, axis=-1, keepdims=True)
                    terms = jnp.where(visible, jnp.exp(scores - peak), 0.0)
                else:
                    last = peaks[m, rows, 0:1]
                    peak = jnp.maximum(last, jnp.max(scores, axis=-1, keepdims=True))
                    terms = jnp.exp(scores - peak)
                total = jnp.sum(terms, axis=-1, keepdims=True)
                acc = jnp.dot(
                    terms.astype(jnp.bfloat16),
                    kv_all[keys, 2 * HD : 4 * HD],
                    preferred_element_type=jnp.float32,
                )
                if not first:
                    fade = jnp.exp(last - peak)
                    total = total + fade * totals[m, rows, 0:1]
                    acc = acc + fade * sums[m, rows, :]
                peaks[m, rows, :] = jnp.broadcast_to(peak, (tok, HD))
                totals[m, rows, :] = jnp.broadcast_to(total, (tok, HD))
                sums[m, rows, :] = acc

    attend(z, True)
    for d in range(1, planes):

        @pl.when(z - d >= 0)
        def _():
            for e in range(plane):
                here = keys_of((z + planes - d) % planes, e)
                remote(here, here, kv_send.at[d, e], kv_recv.at[d, e], below, tp).wait_recv()

                @pl.when(z + 1 < planes)
                def _():
                    remote(
                        here, here, kv_send.at[d + 1, e], kv_recv.at[d + 1, e], above, tp
                    ).start()

        @pl.when(z - d >= 0)
        def _():
            attend((z + planes - d) % planes, False)

        if d == 1:
            pass_weights(0)

    send_weights(False)

    @pl.loop(0, plane)
    def _(chunk):
        rows = block_of(chunk, tok)
        mixed = (
            sums[0, rows, :] / totals[0, rows, 0:1]
            - mix_weight[p] * sums[1, rows, :] / totals[1, rows, 0:1]
        )
        scale = lax.rsqrt(jnp.mean(mixed * mixed, axis=-1, keepdims=True) + epsilon)
        head_out[rows, :] = (mixed * scale * head_gain[...]).astype(jnp.bfloat16)

    own = pltpu.make_async_copy(head_out.at[block_of(p, tok), :], heads.at[p], b_own)
    own.start()
    for d in range(1, plane):
        there = (p + d) % plane
        copy = remote(
            head_out.at[block_of(there, tok), :], heads.at[p],
            b_send.at[d], b_recv.at[d], z * plane + there, tp,
        )
        copy.start()
        started.append(copy)
    own.wait()
    share_weights(planes - 1)
    for d in range(1, plane):
        there = (p + plane - d) % plane
        remote(
            heads.at[there], heads.at[there], b_send.at[d], b_recv.at[d], z * plane + there, tp
        ).wait_recv()

    for copy in loads:
        copy.wait()
    columns = 512

    def product(which, at):
        total = None
        for h in range(plane):
            term = jnp.dot(
                heads[h, block_of(which, half), :],
                out_weight[h * val : (h + 1) * val, at : at + columns],
                preferred_element_type=jnp.float32,
            )
            total = term if total is None else total + term
        return total.astype(jnp.bfloat16)

    model = out_weight.shape[1]
    for at in range(0, model, columns):
        part[:, at : at + columns] = product(other, at)
    swap = remote(part, part_in, t_send, t_recv, sp, other)
    swap.start()
    started.append(swap)
    for at in range(0, model, columns):
        stream[:, at : at + columns] = product(tp, at).astype(jnp.float32)
    swap.wait_recv()
    whole = residual[...].astype(jnp.float32) + (stream[...] + part_in[...].astype(jnp.float32))
    stream[...] = whole
    scaled = whole * lax.rsqrt(jnp.mean(whole * whole, axis=-1, keepdims=True) + epsilon) * gain[...]
    normed[z, block_of(tp, half), :] = scaled.astype(jnp.bfloat16)
    tail[...] = scaled[half - 8 :, :].astype(jnp.bfloat16)

    def tokens(index, which):
        return normed.at[index % planes, block_of(which, half), :]

    mine = tokens(z, tp)

    @pl.when(z + 1 < planes)
    def _():
        remote(mine, mine, up_send.at[1], up_recv.at[1], above, tp).start()

    @pl.when(z > 0)
    def _():
        remote(mine, mine, down_send.at[1], down_recv.at[1], below, tp).start()

    remote(mine, mine, f_send.at[0], f_recv.at[0], sp, other).start()
    after = (p + 1) % plane
    zone = z + (p + 1) // plane

    @pl.when(jnp.logical_and(tp == 1, zone < planes))
    def _():
        for s in range(planes):
            for t in range(2):
                remote(
                    tail, halo.at[zone], h_send.at[s, t], h_recv.at[zone], s * plane + after, t
                ).start()

    for d in range(planes - 2, 0, -1):
        share_weights(d)
        pass_weights(d + 1)
    for d in range(1, planes):

        @pl.when(z - d >= 0)
        def _():
            theirs = tokens(z + planes - d, tp)
            remote(theirs, theirs, up_send.at[d], up_recv.at[d], below, tp).wait_recv()

            @pl.when(z + 1 < planes)
            def _():
                remote(theirs, theirs, up_send.at[d + 1], up_recv.at[d + 1], above, tp).start()

            remote(theirs, theirs, f_send.at[d], f_recv.at[d], sp, other).start()

        @pl.when(z + d < planes)
        def _():
            theirs = tokens(z + d, tp)
            remote(theirs, theirs, down_send.at[d], down_recv.at[d], above, tp).wait_recv()

            @pl.when(z > 0)
            def _():
                remote(theirs, theirs, down_send.at[d + 1], down_recv.at[d + 1], below, tp).start()

            at = planes - d
            remote(theirs, theirs, f_send.at[at], f_recv.at[at], sp, other).start()

    for d in range(planes):
        theirs = tokens(z + planes - d, other)
        remote(theirs, theirs, f_send.at[d], f_recv.at[d], sp, other).wait()
    for s in range(planes):

        @pl.when(s * plane + p > 0)
        def _():
            remote(tail, halo.at[s], h_send.at[s, 0], h_recv.at[s], sp, other).wait_recv()

        @pl.when(s * plane + p == 0)
        def _():
            halo[s] = jnp.zeros(halo.shape[1:], halo.dtype)

    pass_weights(1)
    for copy in own_weights:
        copy.wait()
    for d in range(planes):
        for e in (3,) if square else ():
            there = partner(e)
            rows = block_of((z + planes - d) % planes * plane + there, tok)
            for m, dst in enumerate((lift_all, gate_all)):
                remote(
                    dst.at[rows, :], dst.at[rows, :], g_send.at[d, e, m], g_recv.at[d, e, m],
                    z * plane + there, tp,
                ).wait_recv()

    @pl.when(jnp.logical_and(tp == 1, zone < planes))
    def _():
        for s in range(planes):
            for t in range(2):
                remote(tail, halo.at[0], h_send.at[s, t], h_recv.at[0], sp, other).wait_send()

    for d in range(1, planes):

        @pl.when(jnp.logical_and(z + 1 < planes, z - d + 1 >= 0))
        def _():
            for e in range(plane):
                block = keys_of(z, e)
                remote(block, block, kv_send.at[d, e], kv_recv.at[d, e], above, tp).wait_send()
            remote(mine, mine, up_send.at[d], up_recv.at[d], above, tp).wait_send()

        @pl.when(jnp.logical_and(z > 0, z + d - 1 < planes))
        def _():
            remote(mine, mine, down_send.at[d], down_recv.at[d], below, tp).wait_send()

    for copy in started:
        copy.wait_send()


def down_kernel(
    plane, planes, starts, hidden, weight, stream, out,
    held, units, total, part, part_in, l_sem, own_sem, a_send, a_recv, t_send, t_recv,
):
    sp, tp = lax.axis_index("sp"), lax.axis_index("tp")
    z, p = sp // plane, sp % plane
    other = 1 - tp
    tok, width = units.shape[1:]
    half = tok // 2
    tiles = weight.shape[0] // 128

    def load(d):
        at = (z + planes - d) % planes
        first = pl.multiple_of(at * tiles // planes * 128, 128)
        return pltpu.make_async_copy(weight.at[pl.ds(first, width), :], held.at[d], l_sem.at[d])

    for d in range(planes):
        load(d).start()
    greet([((z + d) % planes * plane + p, tp) for d in range(1, planes)] + [(sp, other)])
    started = []
    own = pltpu.make_async_copy(hidden.at[z], units.at[z], own_sem)
    own.start()
    for d in range(1, planes):
        there = (z + d) % planes
        copy = remote(
            hidden.at[there], units.at[z], a_send.at[d], a_recv.at[d], there * plane + p, tp
        )
        copy.start()
        started.append(copy)
    columns = 512
    order = [0] + list(range(1, planes))
    for d in order:
        there = (z + planes - d) % planes
        load(d).wait()
        if d:
            remote(
                units.at[there], units.at[there], a_send.at[d], a_recv.at[d], sp, other
            ).wait_recv()
        else:
            own.wait()

        @pl.loop(0, weight.shape[1] // columns)
        def _(at):
            here = block_of(at, columns)
            term = jnp.dot(units[there], held[d, :, here], preferred_element_type=jnp.float32)
            total[:, here] = term if d == 0 else total[:, here] + term

    part[...] = total[block_of(other, half), :].astype(jnp.bfloat16)
    swap = remote(part, part_in, t_send, t_recv, sp, other)
    swap.start()
    started.append(swap)
    mine = total[block_of(tp, half), :].astype(jnp.bfloat16).astype(jnp.float32)
    swap.wait_recv()
    out[...] = (stream[...] + (mine + part_in[...].astype(jnp.float32))).astype(out.dtype)
    for copy in started:
        copy.wait_send()


def shorter_routes(
    plane, planes,
    query_one, key_one, query_two, key_two, values, mix_weight, head_gain, residual, out_weight,
    norm_gain, lift_weight, gate_weight, conv_taps, down_weight,
):
    bf16, f32 = jnp.bfloat16, jnp.float32
    tok = query_one.shape[0]
    model = residual.shape[1]
    val = 2 * HD
    ff = lift_weight.shape[1]
    tiles = ff // 128
    starts = [s * tiles // planes * 128 for s in range(planes + 1)]
    width = -(-tiles // planes) * 128
    count = planes * plane * tok
    sp = lax.axis_index("sp")
    z, p = sp // plane, sp % plane
    dma = pltpu.SemaphoreType.DMA
    anywhere = pl.BlockSpec(memory_space=pl.ANY)
    local = pl.BlockSpec(memory_space=pltpu.VMEM)
    shape = jax.ShapeDtypeStruct

    span = plane * tok
    pair = dma((planes + 1,))
    lift_all, gate_all, normed, halo, stream = pl.pallas_call(
        functools.partial(front_kernel, plane, planes, width),
        out_shape=(
            shape((count, width), bf16),
            shape((count, width), bf16),
            shape((planes, tok, model), bf16),
            shape((planes, 8, model), bf16),
            shape((tok // 2, model), f32),
        ),
        in_specs=[anywhere] * 7 + [pl.BlockSpec(memory_space=pltpu.SMEM)] + [local, anywhere, anywhere, local],
        out_specs=(anywhere, anywhere, local, local, local),
        scratch_shapes=[
            pltpu.VMEM((span, 2 * HD), bf16),
            pltpu.VMEM((count, 4 * HD), bf16),
            pltpu.VMEM((2, span, HD), f32),
            pltpu.VMEM((2, span, HD), f32),
            pltpu.VMEM((2, span, val), f32),
            pltpu.VMEM((span, val), bf16),
            pltpu.VMEM((plane, tok, val), bf16),
            pltpu.VMEM((tok // 2, model), bf16),
            pltpu.VMEM((tok // 2, model), bf16),
            pltpu.VMEM((8, model), bf16),
            pltpu.VMEM(out_weight.shape, bf16),
            pltpu.VMEM(residual.shape, bf16),
            dma((9,)), dma((plane, 5)), dma((plane, 5)), dma((planes, 2)), dma((planes, 2)),
            dma((planes + 1, plane)), dma((planes + 1, plane)), dma((planes, plane, 2)), dma((planes, plane, 2)),
            dma, dma((plane,)), dma((plane,)), dma, dma, pair, pair, pair, pair,
            dma((planes,)), dma((planes,)), dma((planes, 2)), dma((planes,)),
        ],
        compiler_params=pltpu.CompilerParams(
            collective_id=0, has_side_effects=True, vmem_limit_bytes=62 << 20
        ),
        name="front",
    )(
        query_one, key_one, query_two, key_two, values, lift_weight, gate_weight, mix_weight,
        head_gain.reshape(1, val), out_weight, residual, norm_gain.reshape(1, model),
    )

    rows = jnp.concatenate([halo, normed], axis=1).reshape(planes * (tok + 8), model)
    lifted = jnp.dot(rows, lift_all, preferred_element_type=f32).astype(bf16)
    gated = jnp.dot(rows, gate_all, preferred_element_type=f32).astype(bf16)
    lifted = lifted.reshape(planes, tok + 8, width)[:, 8:].astype(f32)
    gated = gated.reshape(planes, tok + 8, width).astype(f32)
    taps = lax.dynamic_slice_in_dim(conv_taps, z * tiles // planes * 128, width, 1)
    conv = 0.0
    for index in range(WIDTH):
        at = 8 - (WIDTH - 1) + index
        conv = conv + taps[index] * gated[:, at : at + tok]
    hidden = (jax.nn.silu(conv) * lifted).astype(bf16)
    mine = (z + 1) * tiles // planes * 128 - z * tiles // planes * 128
    hidden = jnp.where(lax.iota(jnp.int32, width) < mine, hidden, 0)

    return pl.pallas_call(
        functools.partial(down_kernel, plane, planes, starts),
        out_shape=shape((tok // 2, model), bf16),
        in_specs=[local, anywhere, local],
        out_specs=local,
        scratch_shapes=[
            pltpu.VMEM((planes, width, model), bf16),
            pltpu.VMEM((planes, tok, width), bf16),
            pltpu.VMEM((tok, model), f32),
            pltpu.VMEM((tok // 2, model), bf16),
            pltpu.VMEM((tok // 2, model), bf16),
            dma((planes,)), dma, dma((planes,)), dma((planes,)), dma, dma,
        ],
        compiler_params=pltpu.CompilerParams(
            collective_id=1, has_side_effects=True, vmem_limit_bytes=62 << 20
        ),
        name="down",
    )(hidden, down_weight, stream)


def any_route(*arrays):
    tok, heads, ff = arrays[0].shape[0], arrays[5].shape[0], arrays[10].shape[1]
    devices, groups = lax.axis_size("sp"), lax.axis_size("tp")
    planes = devices // heads
    fits = (
        groups == 2 and heads > 1 and planes > 1 and devices % heads == 0
        and ff % 128 == 0 and tok % 128 == 0 and WIDTH <= 9
        and arrays[10].shape[0] == tok
    )
    if fits:
        return shorter_routes(heads, planes, *arrays)
    return on_device(*arrays)


def solution(mesh):
    return jax.shard_map(
        any_route,
        mesh=mesh,
        in_specs=(
            P("sp", "tp"),
            P("sp", "tp"),
            P("sp", "tp"),
            P("sp", "tp"),
            P("sp", "tp"),
            P("tp"),
            P(),
            P(("sp", "tp"), None),
            P("tp", None),
            P(),
            P("sp", "tp"),
            P("sp", "tp"),
            P(None, "tp"),
            P("tp", None),
        ),
        out_specs=P(("sp", "tp"), None),
        check_vma=False,
    )
```

profile of v0, /device:TPU:1, one launch (start us, length us, event | category | flops | bytes accessed | tf_op | source)
XLA Modules:
  0.0 150.2 jit_solution(11824747581877721646)
XLA Ops:
  0.0 111.7 %front.1 = (bf16[2048,768]{1,0:T(8,128)(2,1)}, bf16[2048,768]{1,0:T(8,128)(2,1)}, bf16[4,128,2048]{2,1,0:T(8,128)(2,1)}, bf16[4,8,2048]{2,1,0:T(8,128)(2,1)}, f32[64,2048]{1,0:T(8,128)}) custom-call(bf16[128,512]{1,0:T(8,128)(2,1)} %q1.1, bf16[128,512]{1,0:T(8,128)(2,1)} %k1.1, bf16[128,512]{1,0:T(8,128)(2,1)} %q2.1, bf16[128,512]{1,0:T(8,128)(2,1)} %k2.1, ...), custom_call_target="tpu_custom_call" | custom-call | tf_op jit(solution)/shard_map/front/pallas_call | solution.py:628
  111.7 0.0 copy-start.1
  111.7 1.9 %pad_maximum_fusion = bf16[4,136,2048]{2,1,0:T(8,128)(2,1)S(1)} fusion(bf16[4,128,2048]{2,1,0:T(8,128)(2,1)} %get-tuple-element.11, bf16[4,8,2048]{2,1,0:T(8,128)(2,1)} %get-tuple-element.10), kind=kLoop, calls=%fused_computation | loop fusion | flops 4456448 | bytes 4456448 | tf_op jit(solution)/shard_map/concatenate | solution.py:666
  113.6 0.7 copy-done.1
  114.3 0.0 copy-start
  114.3 1.9 %convolution_convert_fusion = bf16[544,768]{1,0:T(8,128)(2,1)S(1)} fusion(bf16[544,2048]{1,0:T(8,128)(2,1)S(1)} %bitcast.10, bf16[2048,768]{1,0:T(8,128)(2,1)S(1)} %copy-done.1), kind=kOutput, calls=%fused_computation.7 | convolution fusion | flops 1711693824 | bytes 6209536 | tf_op jit(solution)/shard_map/dot_general | solution.py:667
  116.2 0.0 copy-done
  116.2 1.9 %convolution_convert_fusion.1 = bf16[544,768]{1,0:T(8,128)(2,1)S(1)} fusion(bf16[544,2048]{1,0:T(8,128)(2,1)S(1)} %bitcast.11, bf16[2048,768]{1,0:T(8,128)(2,1)S(1)} %copy-done), kind=kOutput, calls=%fused_computation.8 | convolution fusion | flops 1711693824 | bytes 6209536 | tf_op jit(solution)/shard_map/dot_general | solution.py:668
  118.1 0.1 convert.1
  118.3 0.9 dynamic-slice_reduce_fusion.2
  119.2 1.8 %broadcast_select_fusion.hidden = bf16[4,128,768]{2,1,0:T(8,128)(2,1)} fusion(pred[768]{0:T(1024)(128)(4,1)S(1)} %iota_compare_fusion, bf16[4,136,768]{2,1,0:T(8,128)(2,1)S(1)} %bitcast.13, f32[4,136,768]{2,1,0:T(8,128)S(1)} %convert.1, f32[768]{0:T(1024)S(1)} %get-tuple-element.17, f32[768]{0:T(1024)S(1)} %get-tuple-element.16, f32[768]{0:T(1024)S(1)} %get-tuple-element.15), kind=kLoop, calls=%fused_computation.9 | loop fusion | flops 5111808 | bytes 6301440 | tf_op jit(solution)/shard_map/jit(_where)/select_n | solution.py:678
  121.0 27.5 %down.1 = bf16[64,2048]{1,0:T(8,128)(2,1)} custom-call(bf16[4,128,768]{2,1,0:T(8,128)(2,1)} %broadcast_select_fusion.hidden, bf16[2816,2048]{1,0:T(8,128)(2,1)} %weight.1, f32[64,2048]{1,0:T(8,128)} %get-tuple-element.14.stream), custom_call_target="tpu_custom_call" | custom-call | tf_op jit(solution)/shard_map/down/pallas_call | solution.py:680
  148.5 1.7 %copy.16 = bf16[64,2048]{1,0:T(8,128)(2,1)} copy(bf16[64,2048]{1,0:T(8,128)(2,1)} %down.1) | data formatting | bytes 524288
  (1 shorter events, 0.0 us)
Async XLA Ops:
  111.7 2.6 %copy-start.1 = (bf16[2048,768]{1,0:T(8,128)(2,1)S(1)}, bf16[2048,768]{1,0:T(8,128)(2,1)}, u32[]{:S(2)}) copy-start(bf16[2048,768]{1,0:T(8,128)(2,1)} %get-tuple-element.13) | copy-start | bytes 9437188
  114.3 1.9 %copy-start = (bf16[2048,768]{1,0:T(8,128)(2,1)S(1)}, bf16[2048,768]{1,0:T(8,128)(2,1)}, u32[]{:S(2)}) copy-start(bf16[2048,768]{1,0:T(8,128)(2,1)} %get-tuple-element.12) | copy-start | bytes 9437188
where the time goes:
time: 152 us; the launch traced here: 150 us
  Pallas kernels  139 us (91%)
  matrix products  3.82 us (3%)
  other arithmetic  3.8 us (2%)
  local copies, waits for them, and re-layouts  3.25 us (2%)
    pallas_call x1, Pallas kernels, shorter_routes(): pl.pallas_call(functools.partial(front_kernel, plane, planes, width), out...  112 us
    pallas_call x1, Pallas kernels, shorter_routes(): pl.pallas_call(functools.partial(down_kernel, plane, planes, starts), out...  27.5 us

commit v1 on v0

v1 whole, which is shorter than its diff:
```python
import functools

import jax
import jax.numpy as jnp
from jax import lax
from jax.experimental import pallas as pl
from jax.experimental.pallas import tpu as pltpu
from jax.sharding import PartitionSpec as P

HD = 128
STRETCH = 64
WIDTH = 3


epsilon = 1e-06
masked_score = -1e30


def passed_along(block, axis, distance):
    devices = range(lax.axis_size(axis))
    route = [(i - distance, i) for i in devices if i - distance in devices]
    return lax.ppermute(block, axis, route)


def update_map(peak, total, acc, queries, keys, vals, visible):
    scores = jnp.einsum("thd,shd->hts", queries, keys, preferred_element_type=jnp.float32) * HD ** (
        -0.5
    )
    scores = jnp.where(visible[None], scores, masked_score)
    new_peak = jnp.maximum(peak, jnp.max(scores, axis=-1))
    weights = jnp.where(visible[None], jnp.exp(scores - new_peak[..., None]), 0.0)
    total = jnp.sum(weights, axis=-1)
    acc = jnp.einsum(
        "hts,she->hte", weights.astype(jnp.bfloat16), vals, preferred_element_type=jnp.float32
    )
    return (new_peak, total, acc)


def on_device(
    query_one,
    key_one,
    query_two,
    key_two,
    values,
    mix_weight,
    head_gain,
    residual,
    out_weight,
    norm_gain,
    lift_weight,
    gate_weight,
    conv_taps,
    down_weight,
):
    tok_local = query_one.shape[0]
    heads_local = mix_weight.shape[0]
    val_width = values.shape[1] // heads_local
    model_width = residual.shape[1]
    offset = lax.axis_index("sp") * tok_local
    q_pos = offset + lax.iota(jnp.int32, tok_local)
    q_one = query_one.reshape(tok_local, heads_local, HD)
    q_two = query_two.reshape(tok_local, heads_local, HD)
    start_peak = jnp.full((heads_local, tok_local), masked_score, jnp.float32)
    start_total = jnp.zeros((heads_local, tok_local), jnp.float32)
    start_acc = jnp.zeros((heads_local, tok_local, val_width), jnp.float32)
    initial = (start_peak, start_total, start_acc, start_peak, start_total, start_acc)
    first_keys = lax.all_gather(key_one, "sp", axis=0, tiled=True)
    second_keys = lax.all_gather(key_two, "sp", axis=0, tiled=True)
    piece_vals = lax.all_gather(values, "sp", axis=0, tiled=True)
    count = first_keys.shape[0]
    k_pos = lax.iota(jnp.int32, count)
    visible = k_pos[None, :] // STRETCH <= q_pos[:, None] // STRETCH
    first_keys = first_keys.reshape(count, heads_local, HD)
    second_keys = second_keys.reshape(count, heads_local, HD)
    piece_vals = piece_vals.reshape(count, heads_local, val_width)
    first = update_map(initial[0], initial[1], initial[2], q_one, first_keys, piece_vals, visible)
    second = update_map(initial[3], initial[4], initial[5], q_two, second_keys, piece_vals, visible)
    state = first + second
    mixed = (
        state[2] / state[1][..., None] - mix_weight[:, None, None] * state[5] / state[4][..., None]
    )
    head_out = (
        mixed * lax.rsqrt(jnp.mean(mixed * mixed, axis=-1, keepdims=True) + epsilon) * head_gain
    ).astype(jnp.bfloat16)
    out_heads = out_weight.reshape(heads_local, val_width, model_width)
    piece = head_out
    attended = lax.psum_scatter(
        jnp.einsum("hte,hed->td", piece, out_heads, preferred_element_type=jnp.float32).astype(
            jnp.bfloat16
        ),
        "tp",
        scatter_dimension=0,
        tiled=True,
    ).astype(jnp.float32)
    stream = residual.astype(jnp.float32) + attended
    normed = (
        stream * lax.rsqrt(jnp.mean(stream * stream, axis=-1, keepdims=True) + epsilon) * norm_gain
    ).astype(jnp.bfloat16)
    whole_rows = lax.all_gather(normed, "tp", axis=0, tiled=True)
    lift_pre = jnp.dot(
        whole_rows,
        lax.all_gather(lift_weight, "sp", axis=0, tiled=True),
        preferred_element_type=jnp.float32,
    )
    gate_pre = jnp.dot(
        whole_rows,
        lax.all_gather(gate_weight, "sp", axis=0, tiled=True),
        preferred_element_type=jnp.float32,
    )
    lifted = lift_pre.astype(jnp.bfloat16)
    gated = gate_pre.astype(jnp.bfloat16)
    prior = passed_along(gated[tok_local - (WIDTH - 1) :], "sp", 1)
    extended = jnp.concatenate([prior, gated], axis=0).astype(jnp.float32)
    conv = conv_taps[0] * extended[0:tok_local]
    for index in range(1, WIDTH):
        conv = conv + conv_taps[index] * extended[index : index + tok_local]
    hidden = (jax.nn.silu(conv) * lifted.astype(jnp.float32)).astype(jnp.bfloat16)
    piece = hidden
    mixer = lax.psum_scatter(
        jnp.dot(piece, down_weight, preferred_element_type=jnp.float32).astype(jnp.bfloat16),
        "tp",
        scatter_dimension=0,
        tiled=True,
    ).astype(jnp.float32)
    return (stream + mixer).astype(jnp.bfloat16)

MESH = pl.DeviceIdType.MESH


def remote(src, dst, send_sem, recv_sem, sp, tp):
    return pltpu.make_async_remote_copy(
        src_ref=src,
        dst_ref=dst,
        send_sem=send_sem,
        recv_sem=recv_sem,
        device_id=(sp, tp),
        device_id_type=MESH,
    )


def block_of(index, size):
    return pl.ds(pl.multiple_of(index * size, size), size)


def layer_kernel(
    plane, planes, width,
    q1, k1, q2, k2, v, lift, gate, mix_weight, head_gain, out_hbm, residual_hbm, gain, taps, down_hbm,
    out,
    q_all, kv_all, head_out, heads, part, part_in, tail, out_weight, residual, stream, piece_out, piece_in,
    lift_all, gate_all, held, normed, gated, hidden, units, total,
    own_sem, a_send, a_recv, k_send, k_recv, w_send, w_recv, g_send, g_recv, l_sem,
    b_own, b_send, b_recv, t_send, t_recv, n_send, n_recv, f_send, f_recv,
    h_send, h_recv, hf_send, hf_recv, u_send, u_recv, y_send, y_recv,
):
    sp, tp = lax.axis_index("sp"), lax.axis_index("tp")
    z, p = sp // plane, sp % plane
    other = 1 - tp
    tok = q1.shape[0]
    half = tok // 2
    val = 2 * HD
    span = plane * tok
    tiles = lift.shape[1] // 128
    model = out_weight.shape[1]
    pad = normed.shape[1] - tok
    before, after = (p + plane - 1) % plane, (p + 1) % plane
    zone = z + (p + 1) // plane
    weights = ((lift, lift_all), (gate, gate_all))

    square = plane == 4
    direct = (1, 2) if square else range(1, plane)

    def flip(index, e):
        return {0: index, 1: index + 1 - 2 * (index % 2), 2: (index + 2) % 4, 3: 3 - index}[e]

    def to_chip(e):
        return flip(p, e) if square else (p + e) % plane

    def from_chip(e):
        return flip(p, e) if square else (p + plane - e) % plane

    def to_plane(d):
        return flip(z, d) if planes == 4 else (z + d) % planes

    def from_plane(d):
        return flip(z, d) if planes == 4 else (z + planes - d) % planes

    peers = (
        [(z * plane + (p + d) % plane, tp) for d in range(1, plane)]
        + [((z + d) % planes * plane + p, tp) for d in range(1, planes)]
        + [(sp, other)]
    )
    barrier = pltpu.get_barrier_semaphore()
    for peer in peers:
        pl.semaphore_signal(barrier, inc=1, device_id=peer, device_id_type=MESH)

    @pl.when(tp == 1)
    def _():
        for s in range(planes):
            pl.semaphore_signal(
                barrier, inc=1, device_id=(s * plane + before, 1), device_id_type=MESH
            )

    def piece(head, row):
        h1, h2 = block_of(head, HD), block_of(head, val)
        rows, own_rows = block_of(row * plane + p, tok), block_of(row, tok)
        return [
            (k1.at[:, h1], kv_all.at[rows, 0:HD]),
            (k2.at[:, h1], kv_all.at[rows, HD : 2 * HD]),
            (v.at[:, h2], kv_all.at[rows, 2 * HD : 4 * HD]),
            (q1.at[:, h1], q_all.at[own_rows, 0:HD]),
            (q2.at[:, h1], q_all.at[own_rows, HD : 2 * HD]),
        ]

    def units_of(index):
        return pl.ds(pl.multiple_of(index * tiles // planes * 128, 128), width)

    own = [
        pltpu.make_async_copy(src, dst, own_sem.at[n]) for n, (src, dst) in enumerate(piece(z, z))
    ]
    own_weights = [
        pltpu.make_async_copy(src.at[:, units_of(z)], dst.at[block_of(sp, tok), :], own_sem.at[5 + m])
        for m, (src, dst) in enumerate(weights)
    ]
    loads = [
        pltpu.make_async_copy(out_hbm, out_weight, own_sem.at[7]),
        pltpu.make_async_copy(residual_hbm, residual, own_sem.at[8]),
    ]

    def load(s):
        first = s * tiles // planes * 128
        return pltpu.make_async_copy(down_hbm.at[first : first + width, :], held.at[s], l_sem.at[s])

    for copy in own:
        copy.start()
    started = []

    def send(copy):
        copy.start()
        started.append(copy)

    pl.semaphore_wait(barrier, len(peers) + planes * tp)

    def exchange(which):
        for d in range(1, planes):
            pairs = piece(to_plane(d), z)
            for n in which:
                src, dst = pairs[n]
                send(remote(src, dst, a_send.at[d, n], a_recv.at[d, n], to_plane(d) * plane + p, tp))

    def exchanged(d, which):
        pairs = piece(z, from_plane(d))
        for n in which:
            src, dst = pairs[n]
            remote(src, dst, a_send.at[d, n], a_recv.at[d, n], sp, other).wait_recv()

    def kv_block(d, m, chip):
        rows = block_of(from_plane(d) * plane + chip, tok)
        return kv_all.at[rows, m * val : (m + 1) * val]

    def weight_block(d, m, chip):
        return weights[m][1].at[block_of(from_plane(d) * plane + chip, tok), :]

    kv = (kv_block, k_send, k_recv)
    wt = (weight_block, g_send, g_recv)

    def spread(kind, d, m, src=None):
        block_at, sends, recvs = kind
        block = block_at(d, m, p)
        for e in direct:
            send(
                remote(
                    block if src is None else src, block, sends.at[d, e, m], recvs.at[d, e, m],
                    z * plane + to_chip(e), tp,
                )
            )

    def arrived(kind, d, e, m):
        block_at, sends, recvs = kind
        block = block_at(d, m, from_chip(e))
        remote(block, block, sends.at[d, e, m], recvs.at[d, e, m], sp, other).wait_recv()

    def relay(kind, d, m):
        block_at, sends, recvs = kind
        for e in direct:
            arrived(kind, d, e, m)
            if square and e == m + 1:
                block = block_at(d, m, from_chip(e))
                send(
                    remote(
                        block, block, sends.at[d, 3, m], recvs.at[d, 3, m],
                        z * plane + to_chip(3 - e), tp,
                    )
                )

    def settle(kind, d, m):
        if square:
            arrived(kind, d, 3, m)

    def send_weights(m):
        for d in range(1, planes):
            src, dst = weights[m]
            send(
                remote(
                    src.at[:, units_of(to_plane(d))], dst.at[block_of(sp, tok), :],
                    w_send.at[d, m], w_recv.at[d, m], to_plane(d) * plane + p, tp,
                )
            )

    def share_weights(d, m):
        if d == 0:
            spread(wt, d, m, weights[m][0].at[:, units_of(z)])
        else:
            block = weight_block(d, m, p)
            remote(block, block, w_send.at[d, m], w_recv.at[d, m], sp, other).wait_recv()
            spread(wt, d, m)

    exchange((0, 1, 2))
    for copy in own[:3]:
        copy.wait()
    for m in range(2):
        spread(kv, 0, m)
    exchange((3, 4))
    share_weights(0, 0)
    send_weights(0)
    for copy in own_weights + loads:
        copy.start()
    for s in range(planes):
        load(s).start()
    for d in range(1, planes):
        exchanged(d, (0, 1, 2))
        for m in range(2):
            spread(kv, d, m)
        for m in range(2):
            relay(kv, d - 1, m)
    for m in range(2):
        relay(kv, planes - 1, m)
    share_weights(0, 1)
    relay(wt, 0, 0)
    for copy in own[3:]:
        copy.wait()
    for d in range(1, planes):
        exchanged(d, (3, 4))
    for d in range(planes):
        for m in range(2):
            settle(kv, d, m)

    for s in range(planes):
        rows, count = slice(s * tok, (s + 1) * tok), (s + 1) * span
        mixed = None
        for m in range(2):
            scores = lax.dot_general(
                q_all[rows, m * HD : (m + 1) * HD],
                kv_all[0:count, m * HD : (m + 1) * HD],
                (((1,), (1,)), ((), ())),
                preferred_element_type=jnp.float32,
            ) * HD ** (-0.5)
            k_pos = lax.broadcasted_iota(jnp.int32, (tok, span), 1)
            q_pos = p * tok + lax.broadcasted_iota(jnp.int32, (tok, span), 0)
            visible = lax.div(k_pos, STRETCH) <= lax.div(q_pos, STRETCH)
            last = jnp.where(visible, scores[:, count - span :], masked_score)
            scores = jnp.concatenate([scores[:, : count - span], last], axis=1) if s else last
            peak = jnp.max(scores, axis=-1, keepdims=True)
            terms = jnp.exp(scores - peak)
            sums = jnp.sum(terms, axis=-1, keepdims=True)
            acc = jnp.dot(
                terms.astype(jnp.bfloat16),
                kv_all[0:count, 2 * HD : 4 * HD],
                preferred_element_type=jnp.float32,
            )
            if m == 0:
                mixed = acc / sums
            else:
                mixed = mixed - mix_weight[z] * acc / sums
        scale = lax.rsqrt(jnp.mean(mixed * mixed, axis=-1, keepdims=True) + epsilon)
        head_out[s] = (mixed * scale * head_gain[...]).astype(jnp.bfloat16)

        @pl.when(z != s)
        def _():
            remote(
                head_out.at[s], heads.at[z], b_send.at[s], b_recv.at[z], s * plane + p, tp
            ).start()

        @pl.when(z == s)
        def _():
            pltpu.make_async_copy(head_out.at[s], heads.at[z], b_own).start()

    send_weights(1)
    for m in range(2):
        if m == 0:
            for d in range(1, planes):
                share_weights(d, 0)
        else:
            relay(wt, 0, 1)
    for d in range(1, planes):
        relay(wt, d, 0)
    for s in range(planes):

        @pl.when(z != s)
        def _():
            remote(
                heads.at[s], heads.at[s], b_send.at[s], b_recv.at[s], sp, other
            ).wait_recv()

        @pl.when(z == s)
        def _():
            pltpu.make_async_copy(head_out.at[s], heads.at[s], b_own).wait()

    for copy in loads:
        copy.wait()
    columns = 512

    def product(which, at):
        sums = None
        for h in range(planes):
            term = jnp.dot(
                heads[h, block_of(which, half), :],
                out_weight[h * val : (h + 1) * val, at : at + columns],
                preferred_element_type=jnp.float32,
            )
            sums = term if sums is None else sums + term
        return sums.astype(jnp.bfloat16)

    for at in range(0, model, columns):
        part[:, at : at + columns] = product(other, at)
    swap = remote(part, part_in, t_send, t_recv, sp, other)
    send(swap)
    for at in range(0, model, columns):
        stream[:, at : at + columns] = product(tp, at).astype(jnp.float32)
    swap.wait_recv()
    whole = residual[...].astype(jnp.float32) + (stream[...] + part_in[...].astype(jnp.float32))
    stream[...] = whole
    scaled = whole * lax.rsqrt(jnp.mean(whole * whole, axis=-1, keepdims=True) + epsilon) * gain[...]

    def tokens(s, which):
        return normed.at[s, pl.ds(pl.multiple_of(pad + which * half, 8), half), :]

    normed[z, pl.ds(pl.multiple_of(pad + tp * half, 8), half), :] = scaled.astype(jnp.bfloat16)
    tail[...] = scaled[half - pad :, :].astype(jnp.bfloat16)
    mine = tokens(z, tp)
    for d in range(1, planes):
        send(remote(mine, mine, n_send.at[d], n_recv.at[d], to_plane(d) * plane + p, tp))
    send(remote(mine, mine, f_send.at[0], f_recv.at[0], sp, other))

    @pl.when(jnp.logical_and(tp == 1, zone < planes))
    def _():
        for s in range(planes):
            remote(
                tail, normed.at[zone, 0:pad, :], h_send.at[s], h_recv.at[zone], s * plane + after, 1
            ).start()

    for d in range(1, planes):
        share_weights(d, 1)
    for d in range(1, planes):
        theirs = tokens(from_plane(d), tp)
        remote(theirs, theirs, n_send.at[d], n_recv.at[d], sp, other).wait_recv()
        send(remote(theirs, theirs, f_send.at[d], f_recv.at[d], sp, other))
    for s in range(planes):
        rows = normed.at[s, 0:pad, :]

        @pl.when(s * plane + p > 0)
        def _():
            @pl.when(tp == 1)
            def _():
                remote(rows, rows, h_send.at[s], h_recv.at[s], sp, other).wait_recv()
                remote(rows, rows, hf_send.at[s], hf_recv.at[s], sp, other).start()

            @pl.when(tp == 0)
            def _():
                remote(rows, rows, hf_send.at[s], hf_recv.at[s], sp, other).wait_recv()

        @pl.when(s * plane + p == 0)
        def _():
            normed[s, 0:pad, :] = jnp.zeros((pad, model), jnp.bfloat16)

    for d in range(1, planes):
        relay(wt, d, 1)
    for copy in own_weights:
        copy.wait()
    for m in range(2):
        for d in range(planes):
            settle(wt, d, m)

    first = z * tiles // planes * 128
    mine_units = (z + 1) * tiles // planes * 128 - first
    chunk = 256 if width % 256 == 0 else 128
    for d in range(planes):
        s = from_plane(d)
        theirs = tokens(s, other)
        remote(theirs, theirs, f_send.at[d], f_recv.at[d], sp, other).wait_recv()

        @pl.loop(0, width // chunk)
        def _(at):
            here = block_of(at, chunk)
            gated[...] = (
                jnp.dot(normed[s], gate_all[:, here], preferred_element_type=jnp.float32)
                .astype(jnp.bfloat16)
                .astype(jnp.float32)
            )
            lifted = (
                jnp.dot(normed[s, pad:, :], lift_all[:, here], preferred_element_type=jnp.float32)
                .astype(jnp.bfloat16)
                .astype(jnp.float32)
            )
            lanes = pl.ds(pl.multiple_of(first + at * chunk, 128), chunk)
            conv = None
            for index in range(WIDTH):
                start = pad - (WIDTH - 1) + index
                term = taps[index : index + 1, lanes] * gated[start : start + tok, :]
                conv = term if conv is None else conv + term
            inside = at * chunk + lax.broadcasted_iota(jnp.int32, (tok, chunk), 1) < mine_units
            hidden[s, :, here] = jnp.where(inside, jax.nn.silu(conv) * lifted, 0.0).astype(
                jnp.bfloat16
            )

        if d:
            send(remote(hidden.at[s], units.at[z], u_send.at[d], u_recv.at[d], s * plane + p, tp))

    for d in range(planes):
        s = from_plane(d)
        if d == 0:
            for n in range(planes):
                load(n).wait()
        else:
            remote(units.at[s], units.at[s], u_send.at[d], u_recv.at[d], sp, other).wait_recv()

        @pl.loop(0, model // columns)
        def _(at):
            here = block_of(at, columns)
            block = hidden[s] if d == 0 else units[s]
            term = jnp.dot(block, held[s, :, here], preferred_element_type=jnp.float32)
            total[:, here] = term if d == 0 else total[:, here] + term

    piece_out[...] = total[block_of(other, half), :].astype(jnp.bfloat16)
    swap = remote(piece_out, piece_in, y_send, y_recv, sp, other)
    send(swap)
    near = total[block_of(tp, half), :].astype(jnp.bfloat16).astype(jnp.float32)
    swap.wait_recv()
    out[...] = (stream[...] + (near + piece_in[...].astype(jnp.float32))).astype(out.dtype)

    for s in range(planes):

        @pl.when(z != s)
        def _():
            remote(
                head_out.at[s], heads.at[z], b_send.at[s], b_recv.at[z], s * plane + p, tp
            ).wait_send()

        @pl.when(jnp.logical_and(tp == 1, s * plane + p > 0))
        def _():
            rows = normed.at[s, 0:pad, :]
            remote(rows, rows, hf_send.at[s], hf_recv.at[s], sp, other).wait_send()

        @pl.when(jnp.logical_and(tp == 1, zone < planes))
        def _():
            remote(
                tail, normed.at[s, 0:pad, :], h_send.at[s], h_recv.at[s], s * plane + after, 1
            ).wait_send()

    for copy in started:
        copy.wait_send()


def shorter_routes(
    plane, planes,
    query_one, key_one, query_two, key_two, values, mix_weight, head_gain, residual, out_weight,
    norm_gain, lift_weight, gate_weight, conv_taps, down_weight,
):
    bf16, f32 = jnp.bfloat16, jnp.float32
    tok = query_one.shape[0]
    model = residual.shape[1]
    val = 2 * HD
    tiles = lift_weight.shape[1] // 128
    width = -(-tiles // planes) * 128
    chunk = 256 if width % 256 == 0 else 128
    count = planes * plane * tok
    half = tok // 2
    pad = 8
    dma = pltpu.SemaphoreType.DMA
    anywhere = pl.BlockSpec(memory_space=pl.ANY)
    local = pl.BlockSpec(memory_space=pltpu.VMEM)
    scalars = pl.BlockSpec(memory_space=pltpu.SMEM)
    each = dma((planes,))
    return pl.pallas_call(
        functools.partial(layer_kernel, plane, planes, width),
        out_shape=jax.ShapeDtypeStruct((half, model), bf16),
        in_specs=[anywhere] * 7 + [scalars, local, anywhere, anywhere, local, local, anywhere],
        out_specs=local,
        scratch_shapes=[
            pltpu.VMEM((planes * tok, 2 * HD), bf16),
            pltpu.VMEM((count, 4 * HD), bf16),
            pltpu.VMEM((planes, tok, val), bf16),
            pltpu.VMEM((planes, tok, val), bf16),
            pltpu.VMEM((half, model), bf16),
            pltpu.VMEM((half, model), bf16),
            pltpu.VMEM((pad, model), bf16),
            pltpu.VMEM(out_weight.shape, bf16),
            pltpu.VMEM(residual.shape, bf16),
            pltpu.VMEM((half, model), f32),
            pltpu.VMEM((half, model), bf16),
            pltpu.VMEM((half, model), bf16),
            pltpu.VMEM((count, width), bf16),
            pltpu.VMEM((count, width), bf16),
            pltpu.VMEM((planes, width, model), bf16),
            pltpu.VMEM((planes, pad + tok, model), bf16),
            pltpu.VMEM((pad + tok, chunk), f32),
            pltpu.VMEM((planes, tok, width), bf16),
            pltpu.VMEM((planes, tok, width), bf16),
            pltpu.VMEM((tok, model), f32),
            dma((9,)), dma((planes, 5)), dma((planes, 5)),
            dma((planes, plane, 2)), dma((planes, plane, 2)),
            dma((planes, 2)), dma((planes, 2)),
            dma((planes, plane, 2)), dma((planes, plane, 2)), each,
            dma, each, each, dma, dma, each, each, each, each,
            each, each, each, each, each, each, dma, dma,
        ],
        compiler_params=pltpu.CompilerParams(
            collective_id=0, has_side_effects=True, vmem_limit_bytes=62 << 20
        ),
        name="layer",
    )(
        query_one, key_one, query_two, key_two, values, lift_weight, gate_weight, mix_weight,
        head_gain.reshape(1, val), out_weight, residual, norm_gain.reshape(1, model), conv_taps,
        down_weight,
    )


def any_route(*arrays):
    tok, heads, ff = arrays[0].shape[0], arrays[5].shape[0], arrays[10].shape[1]
    devices, groups = lax.axis_size("sp"), lax.axis_size("tp")
    fits = (
        groups == 2 and heads > 1 and devices > heads and devices % heads == 0
        and ff % 128 == 0 and tok % 128 == 0 and WIDTH <= 9
        and arrays[10].shape[0] == tok
    )
    if fits:
        return shorter_routes(devices // heads, heads, *arrays)
    return on_device(*arrays)


def solution(mesh):
    return jax.shard_map(
        any_route,
        mesh=mesh,
        in_specs=(
            P("sp", "tp"),
            P("sp", "tp"),
            P("sp", "tp"),
            P("sp", "tp"),
            P("sp", "tp"),
            P("tp"),
            P(),
            P(("sp", "tp"), None),
            P("tp", None),
            P(),
            P("sp", "tp"),
            P("sp", "tp"),
            P(None, "tp"),
            P("tp", None),
        ),
        out_specs=P(("sp", "tp"), None),
        check_vma=False,
    )
```

time: 152 us -> 132 us (0.87)
  Pallas kernels: 139 us -> 130 us
  matrix products: 3.82 us -> 0 us
  other arithmetic: 3.8 us -> 0 us
  local copies, waits for them, and re-layouts: 3.25 us -> 1.67 us
    pallas_call x2 -> x1, Pallas kernels: 139 us -> 130 us  [shorter_routes(): pl.pallas_call(functools.partial(layer_kernel, plane, planes, width), out...]
    dot_general x2 -> x0, matrix products: 3.82 us -> none  [the longest x1 1.92 us: shorter_routes(): gated = jnp.dot(rows, gate_all, preferred_element_type=f32).astype(bf16)]
    concatenate x1 -> x0, other arithmetic: 1.9 us -> none  [shorter_routes(): jnp.concatenate([halo, normed], axis=1).reshape(planes * (tok + 8), model)]
    select_n x1 -> x0, other arithmetic: 1.78 us -> none  [shorter_routes(): hidden = jnp.where(lax.iota(jnp.int32, width) < mine, hidden, 0)]
where the time goes in v1:
time: 132 us
  Pallas kernels  130 us (98%)
  local copies, waits for them, and re-layouts  1.67 us (1%)
    pallas_call x1, Pallas kernels, shorter_routes(): pl.pallas_call(functools.partial(layer_kernel, plane, planes, width), out...  130 us

profile of v1, /device:TPU:1, one launch (start us, length us, event | category | flops | bytes accessed | tf_op | source)
XLA Modules:
  0.0 131.7 jit_solution(3496453265095262980)
XLA Ops:
  0.0 130.0 %layer.1 = bf16[64,2048]{1,0:T(8,128)(2,1)} custom-call(bf16[128,512]{1,0:T(8,128)(2,1)} %q1.1, bf16[128,512]{1,0:T(8,128)(2,1)} %k1.1, bf16[128,512]{1,0:T(8,128)(2,1)} %q2.1, bf16[128,512]{1,0:T(8,128)(2,1)} %k2.1, bf16[128,1024]{1,0:T(8,128)(2,1)} %v.1, bf16[128,2816]{1,0:T(8,128)(2,1)} %lift.1, bf16[128,2816]{1,0:T(8,128)(2,1)} %gate.1, f32[4]{0:T(128)} %mix_weight.1, ...), custom_call_target="tpu_custom_call" | custom-call | tf_op jit(solution)/shard_map/layer/pallas_call | solution.py:583
  130.0 1.7 %copy.16 = bf16[64,2048]{1,0:T(8,128)(2,1)} copy(bf16[64,2048]{1,0:T(8,128)(2,1)} %layer.1) | data formatting | bytes 524288

commit v2 on v1

--- a/solution.py
+++ b/solution.py
@@ -165,6 +165,7 @@
     before, after = (p + plane - 1) % plane, (p + 1) % plane
     zone = z + (p + 1) // plane
     weights = ((lift, lift_all), (gate, gate_all))
+    widths = sorted({(s + 1) * tiles // planes - s * tiles // planes for s in range(planes)})
 
     square = plane == 4
     direct = (1, 2) if square else range(1, plane)
@@ -189,6 +190,9 @@
         + [((z + d) % planes * plane + p, tp) for d in range(1, planes)]
         + [(sp, other)]
     )
+    if len(widths) > 1:
+        spare = widths[0] * 128
+        units[:, :, spare:] = jnp.zeros((planes, tok, width - spare), jnp.bfloat16)
     barrier = pltpu.get_barrier_semaphore()
     for peer in peers:
         pl.semaphore_signal(barrier, inc=1, device_id=peer, device_id_type=MESH)
@@ -211,8 +215,17 @@
             (q2.at[:, h1], q_all.at[own_rows, HD : 2 * HD]),
         ]
 
-    def units_of(index):
-        return pl.ds(pl.multiple_of(index * tiles // planes * 128, 128), width)
+
+    def units_of(index, size=width):
+        return pl.ds(pl.multiple_of(index * tiles // planes * 128, 128), size)
+
+    def by_width(index, act):
+        wide = (index + 1) * tiles // planes - index * tiles // planes
+        for count in widths:
+            if len(widths) == 1:
+                act(count * 128)
+            else:
+                pl.when(wide == count)(functools.partial(act, count * 128))
 
     own = [
         pltpu.make_async_copy(src, dst, own_sem.at[n]) for n, (src, dst) in enumerate(piece(z, z))
@@ -232,11 +245,15 @@
 
     for copy in own:
         copy.start()
-    started = []
+    started, sized = [], []
 
     def send(copy):
         copy.start()
         started.append(copy)
+
+    def send_sized(index, make):
+        by_width(index, lambda size: make(size).start())
+        sized.append((index, make))
 
     pl.semaphore_wait(barrier, len(peers) + planes * tp)
 
@@ -253,44 +270,55 @@
             src, dst = pairs[n]
             remote(src, dst, a_send.at[d, n], a_recv.at[d, n], sp, other).wait_recv()
 
-    def kv_block(d, m, chip):
+    def kv_block(d, m, chip, size):
         rows = block_of(from_plane(d) * plane + chip, tok)
         return kv_all.at[rows, m * val : (m + 1) * val]
 
-    def weight_block(d, m, chip):
-        return weights[m][1].at[block_of(from_plane(d) * plane + chip, tok), :]
-
-    kv = (kv_block, k_send, k_recv)
-    wt = (weight_block, g_send, g_recv)
+    def weight_block(d, m, chip, size):
+        return weights[m][1].at[block_of(from_plane(d) * plane + chip, tok), 0:size]
+
+    def plain(index, make):
+        send(make(width))
+
+    kv = (kv_block, k_send, k_recv, plain, lambda index, act: act(width))
+    wt = (weight_block, g_send, g_recv, send_sized, by_width)
 
     def spread(kind, d, m, src=None):
-        block_at, sends, recvs = kind
-        block = block_at(d, m, p)
+        block_at, sends, recvs, start, _ = kind
         for e in direct:
-            send(
-                remote(
-                    block if src is None else src, block, sends.at[d, e, m], recvs.at[d, e, m],
-                    z * plane + to_chip(e), tp,
+
+            def make(size, e=e):
+                block = block_at(d, m, p, size)
+                return remote(
+                    block if src is None else src(size), block,
+                    sends.at[d, e, m], recvs.at[d, e, m], z * plane + to_chip(e), tp,
                 )
-            )
+
+            start(z, make)
 
     def arrived(kind, d, e, m):
-        block_at, sends, recvs = kind
-        block = block_at(d, m, from_chip(e))
-        remote(block, block, sends.at[d, e, m], recvs.at[d, e, m], sp, other).wait_recv()
+        block_at, sends, recvs, _, each_size = kind
+
+        def wait(size):
+            block = block_at(d, m, from_chip(e), size)
+            remote(block, block, sends.at[d, e, m], recvs.at[d, e, m], sp, other).wait_recv()
+
+        each_size(z, wait)
 
     def relay(kind, d, m):
-        block_at, sends, recvs = kind
+        block_at, sends, recvs, start, _ = kind
         for e in direct:
             arrived(kind, d, e, m)
             if square and e == m + 1:
-                block = block_at(d, m, from_chip(e))
-                send(
-                    remote(
+
+                def make(size, e=e):
+                    block = block_at(d, m, from_chip(e), size)
+                    return remote(
                         block, block, sends.at[d, 3, m], recvs.at[d, 3, m],
                         z * plane + to_chip(3 - e), tp,
                     )
-                )
+
+                start(z, make)
 
     def settle(kind, d, m):
         if square:
@@ -299,20 +327,26 @@
     def send_weights(m):
         for d in range(1, planes):
             src, dst = weights[m]
-            send(
-                remote(
-                    src.at[:, units_of(to_plane(d))], dst.at[block_of(sp, tok), :],
+
+            def make(size, d=d):
+                return remote(
+                    src.at[:, units_of(to_plane(d), size)], dst.at[block_of(sp, tok), 0:size],
                     w_send.at[d, m], w_recv.at[d, m], to_plane(d) * plane + p, tp,
                 )
-            )
+
+            send_sized(to_plane(d), make)
 
     def share_weights(d, m):
         if d == 0:
-            spread(wt, d, m, weights[m][0].at[:, units_of(z)])
-        else:
-            block = weight_block(d, m, p)
+            spread(wt, d, m, lambda size: weights[m][0].at[:, units_of(z, size)])
+            return
+
+        def wait(size):
+            block = weight_block(d, m, p, size)
             remote(block, block, w_send.at[d, m], w_recv.at[d, m], sp, other).wait_recv()
-            spread(wt, d, m)
+
+        by_width(z, wait)
+        spread(wt, d, m)
 
     exchange((0, 1, 2))
     for copy in own[:3]:
@@ -451,10 +485,14 @@
     for d in range(1, planes):
         share_weights(d, 1)
     for d in range(1, planes):
-        theirs = tokens(from_plane(d), tp)
-        remote(theirs, theirs, n_send.at[d], n_recv.at[d], sp, other).wait_recv()
-        send(remote(theirs, theirs, f_send.at[d], f_recv.at[d], sp, other))
-    for s in range(planes):
+        relay(wt, d, 1)
+
+    def pass_tokens(d):
+        if d:
+            theirs = tokens(from_plane(d), tp)
+            remote(theirs, theirs, n_send.at[d], n_recv.at[d], sp, other).wait_recv()
+            send(remote(theirs, theirs, f_send.at[d], f_recv.at[d], sp, other))
+        s = from_plane(d)
         rows = normed.at[s, 0:pad, :]
 
         @pl.when(s * plane + p > 0)
@@ -472,8 +510,7 @@
         def _():
             normed[s, 0:pad, :] = jnp.zeros((pad, model), jnp.bfloat16)
 
-    for d in range(1, planes):
-        relay(wt, d, 1)
+    pass_tokens(0)
     for copy in own_weights:
         copy.wait()
     for m in range(2):
@@ -485,6 +522,8 @@
     chunk = 256 if width % 256 == 0 else 128
     for d in range(planes):
         s = from_plane(d)
+        if d + 1 < planes:
+            pass_tokens(d + 1)
         theirs = tokens(s, other)
         remote(theirs, theirs, f_send.at[d], f_recv.at[d], sp, other).wait_recv()
 
@@ -513,7 +552,14 @@
             )
 
         if d:
-            send(remote(hidden.at[s], units.at[z], u_send.at[d], u_recv.at[d], s * plane + p, tp))
+
+            def make(size, s=s, d=d):
+                return remote(
+                    hidden.at[s, :, 0:size], units.at[z, :, 0:size],
+                    u_send.at[d], u_recv.at[d], s * plane + p, tp,
+                )
+
+            send_sized(z, make)
 
     for d in range(planes):
         s = from_plane(d)
@@ -521,7 +567,12 @@
             for n in range(planes):
                 load(n).wait()
         else:
-            remote(units.at[s], units.at[s], u_send.at[d], u_recv.at[d], sp, other).wait_recv()
+
+            def wait(size, s=s, d=d):
+                block = units.at[s, :, 0:size]
+                remote(block, block, u_send.at[d], u_recv.at[d], sp, other).wait_recv()
+
+            by_width(s, wait)
 
         @pl.loop(0, model // columns)
         def _(at):
@@ -558,6 +609,8 @@
 
     for copy in started:
         copy.wait_send()
+    for index, make in sized:
+        by_width(index, lambda size: make(size).wait_send())
 
 
 def shorter_routes(

time: 132 us -> 117 us (0.89)
  Pallas kernels: 130 us -> 115 us
    pallas_call x1, Pallas kernels: 130 us -> 115 us  [shorter_routes(): pl.pallas_call(functools.partial(layer_kernel, plane, planes, width), out...]
where the time goes in v2:
time: 117 us; the launch traced here: 116 us
  Pallas kernels  115 us (98%)
  local copies, waits for them, and re-layouts  1.67 us (1%)
    pallas_call x1, Pallas kernels, shorter_routes(): pl.pallas_call(functools.partial(layer_kernel, plane, planes, width), out...  115 us

profile of v2, /device:TPU:1, one launch (start us, length us, event | category | flops | bytes accessed | tf_op | source)
XLA Modules:
  0.0 116.5 jit_solution(7530563092927654584)
XLA Ops:
  0.0 114.8 %layer.1 = bf16[64,2048]{1,0:T(8,128)(2,1)} custom-call(bf16[128,512]{1,0:T(8,128)(2,1)} %q1.1, bf16[128,512]{1,0:T(8,128)(2,1)} %k1.1, bf16[128,512]{1,0:T(8,128)(2,1)} %q2.1, bf16[128,512]{1,0:T(8,128)(2,1)} %k2.1, bf16[128,1024]{1,0:T(8,128)(2,1)} %v.1, bf16[128,2816]{1,0:T(8,128)(2,1)} %lift.1, bf16[128,2816]{1,0:T(8,128)(2,1)} %gate.1, f32[4]{0:T(128)} %mix_weight.1, ...), custom_call_target="tpu_custom_call" | custom-call | tf_op jit(solution)/shard_map/layer/pallas_call | solution.py:636
  114.8 1.7 %copy.16 = bf16[64,2048]{1,0:T(8,128)(2,1)} copy(bf16[64,2048]{1,0:T(8,128)(2,1)} %layer.1) | data formatting | bytes 524288
